TPU v7x, 32 devices: a whole 2x2x4 slice. The times are simulated.
32 devices in a mesh: fs: 8 (over z, x), tp: 4 (over y, core).
Axes of the slice: x: 2, y: 2, z: 4, core: 2. Of those that a mesh axis runs over, the one named last changes fastest.
Arguments:
- tokens: bfloat16 [4096, 2048], P(('fs', 'tp')), may hold values from -6 to 6
- norm_gain: float32 [2048], replicated, may hold values from 0.1 to 1.9
- up_weight: bfloat16 [2048, 8192], P('fs', 'tp'), may hold values from -0.125 to 0.125
- down_weight: bfloat16 [8192, 2048], P('tp', 'fs'), may hold values from -0.0625 to 0.0625
Outputs:
- mixed: bfloat16 [4096, 2048], P(('fs', 'tp'))
All inputs are finite; a program needn't handle non-finite values.
Results may differ from a plain program's by a relative error of at most 0.013.
Values may be sent and summed in bfloat16 or wider, within the bound.
A program may use at most 64 MiB of HBM per device.

v0:
```python
import jax
import jax.numpy as jnp
from jax import lax
from jax.sharding import PartitionSpec as P

epsilon = 1e-06


def squared_relu(preact):
    return jnp.square(jnp.maximum(preact, 0.0)).astype(jnp.bfloat16)


def expand_rows(normed, up_whole):
    return squared_relu(
        jnp.dot(
            lax.all_gather(normed, "tp", axis=0, tiled=True),
            up_whole,
            preferred_element_type=jnp.float32,
        )
    )


def collect_down(down_weight):
    return lax.all_gather(down_weight, "fs", axis=1, tiled=True)


def on_device(tokens, norm_gain, up_weight, down_weight):
    values = tokens.astype(jnp.float32)
    mean_square = jnp.mean(values * values, axis=-1, keepdims=True)
    normed = (values * lax.rsqrt(mean_square + epsilon) * norm_gain).astype(jnp.bfloat16)
    up_whole = lax.all_gather(up_weight, "fs", axis=0, tiled=True)
    hidden = expand_rows(normed, up_whole)
    down_whole = collect_down(down_weight)
    partial_value = jnp.dot(hidden, down_whole, preferred_element_type=jnp.float32).astype(
        jnp.bfloat16
    )
    partial_value = lax.optimization_barrier(partial_value)
    summed = lax.psum_scatter(
        partial_value.astype(jnp.float32).astype(jnp.bfloat16),
        "tp",
        scatter_dimension=0,
        tiled=True,
    )
    return summed


def solution(mesh):
    placed = (P(("fs", "tp"), None), P(), P("fs", "tp"), P("tp", "fs"))
    return jax.shard_map(
        on_device, mesh=mesh, in_specs=placed, out_specs=P(("fs", "tp"), None), check_vma=False
    )
```

profile of v0, /device:TPU:0, one launch (start us, length us, event | category | flops | bytes accessed | tf_op | source)
XLA Modules:
  0.0 339.7 jit_solution(12480029931812060435)
XLA Ops:
  6.5 0.0 all-gather.4.cloned.1.call-start
  6.5 1.2 fusion
  7.8 2.0 fusion.2
  9.8 0.0 all-gather.4.cloned.1.call-update
  9.8 0.0 all-gather.6.cloned.1.call-start
  9.9 0.7 all-gather.6.cloned.1.call-update
  10.6 0.0 all-gather.8.cloned.1.call-start
  10.6 0.7 all-gather.8.cloned.1.call-update
  11.3 0.0 reduce-scatter.2.cloned.1.call-start
  11.4 23.9 %all-gather.4.cloned.1.call-done = bf16[512,2048]{1,0:T(8,128)(2,1)} async-done(((bf16[128,2048]{1,0:T(8,128)(2,1)}), bf16[512,2048]{1,0:T(8,128)(2,1)}) %all-gather.4.cloned.1.call-update) | async-done | bytes 2097168 | tf_op jit(solution)/shard_map/all_gather | solution.py:16
  35.3 126.6 %all-gather.6.cloned.1.call-done = bf16[2048,2048]{1,0:T(8,128)(2,1)} async-done(((bf16[256,2048]{1,0:T(8,128)(2,1)}), bf16[2048,2048]{1,0:T(8,128)(2,1)}) %all-gather.6.cloned.1.call-update) | async-done | bytes 8388624 | tf_op jit(solution)/shard_map/all_gather | solution.py:31
  161.9 125.2 %all-gather.8.cloned.1.call-done = bf16[2048,2048]{1,0:T(8,128)(2,1)} async-done(((bf16[2048,256]{1,0:T(8,128)(2,1)}), bf16[2048,2048]{1,0:T(8,128)(2,1)}) %all-gather.8.cloned.1.call-update) | async-done | bytes 8388624 | tf_op jit(solution)/shard_map/all_gather | solution.py:24
  287.1 16.5 %convolution_convert_fusion = bf16[512,2048]{1,0:T(8,128)(2,1)} fusion(bf16[2048,2048]{1,0:T(8,128)(2,1)} %all-gather.8.cloned.1.call-done, bf16[512,2048]{1,0:T(8,128)(2,1)} %all-gather.4.cloned.1.call-done, bf16[2048,2048]{1,0:T(8,128)(2,1)} %all-gather.6.cloned.1.call-done), kind=kOutput, calls=%fused_computation.1 | convolution fusion | flops 8594128896 | bytes 20971520 | tf_op jit(solution)/shard_map/dot_general | solution.py:34
  303.6 0.0 reduce-scatter.2.cloned.1.call-update
  303.6 29.5 %reduce-scatter.2.cloned.1.call-done = bf16[128,2048]{1,0:T(8,128)(2,1)} async-done(((bf16[512,2048]{1,0:T(8,128)(2,1)}), bf16[128,2048]{1,0:T(8,128)(2,1)}) %reduce-scatter.2.cloned.1.call-update) | async-done | bytes 524304 | tf_op jit(solution)/shard_map/reduce_scatter | solution.py:38
  (1 shorter events, 0.0 us)
Async XLA Ops:
  6.5 28.7 %all-gather.4.cloned.1.call-start = ((), (), s32[]{:S(2)}) async-start(), calls=%async_computation.1 | async-start | bytes 2621440 | tf_op jit(solution)/shard_map/all_gather | solution.py:16
  9.8 152.1 %all-gather.6.cloned.1.call-start = ((), (), s32[]{:S(2)}) async-start(), calls=%async_computation.2 | async-start | bytes 9437184 | tf_op jit(solution)/shard_map/all_gather | solution.py:31
  10.6 276.5 %all-gather.8.cloned.1.call-start = ((), (), s32[]{:S(2)}) async-start(), calls=%async_computation.3 | async-start | bytes 9437184 | tf_op jit(solution)/shard_map/all_gather | solution.py:24
  11.3 321.8 %reduce-scatter.2.cloned.1.call-start = ((), (), s32[]{:S(2)}) async-start(), calls=%async_computation.4 | async-start | bytes 2621440 | tf_op jit(solution)/shard_map/reduce_scatter | solution.py:38
Sparse Core Ops, SparseCore 0:
  9.9 25.2 all-gather.3
  37.4 124.4 all-gather.5
  163.9 123.1 all-gather.7
  303.7 29.3 reduce-scatter.1
where the time goes:
time: 340 us
  waiting for transfers between devices  307 us (90%)
  matrix products  16.5 us (5%)
  between operations  13.1 us (4%)
    all_gather x1, waiting for transfers between devices, on_device(): up_whole = lax.all_gather(up_weight, 'fs', axis=0, tiled=True)  127 us
    all_gather x1, waiting for transfers between devices, collect_down(): return lax.all_gather(down_weight, 'fs', axis=1, tiled=True)  125 us
    reduce_scatter x1, waiting for transfers between devices, on_device(): lax.psum_scatter(partial_value.astype(jnp.float32).astype(jnp.bfloat16),...  29.5 us
    all_gather x1, waiting for transfers between devices, expand_rows(): lax.all_gather(normed, 'tp', axis=0, tiled=True)  23.9 us
    dot_general x1, matrix products, on_device(): jnp.dot(hidden, down_whole, preferred_element_type=jnp.float32)  16.5 us
  transfers between devices with their start and end apart: 4, of which 4 were waited for; matrix products, arithmetic and copies ran while one was open for 0% of the time, Pallas kernels for 0%

commit v1 on v0

v1 whole, which is shorter than its diff:
```python
import functools
import math

import jax
import jax.numpy as jnp
from jax import lax
from jax.experimental import pallas as pl
from jax.experimental.pallas import tpu as pltpu
from jax.sharding import PartitionSpec as P

epsilon = 1e-06
MESH = pl.DeviceIdType.MESH
f32, bf16 = jnp.float32, jnp.bfloat16


def plain(tokens, norm_gain, up_weight, down_weight):
    values = tokens.astype(f32)
    mean_square = jnp.mean(values * values, axis=-1, keepdims=True)
    normed = (values * lax.rsqrt(mean_square + epsilon) * norm_gain).astype(bf16)
    up_whole = lax.all_gather(up_weight, "fs", axis=0, tiled=True)
    rows = lax.all_gather(normed, "tp", axis=0, tiled=True)
    preact = jnp.dot(rows, up_whole, preferred_element_type=f32)
    hidden = jnp.square(jnp.maximum(preact, 0.0)).astype(bf16)
    down_whole = lax.all_gather(down_weight, "fs", axis=1, tiled=True)
    partial_value = jnp.dot(hidden, down_whole, preferred_element_type=f32).astype(bf16)
    return lax.psum_scatter(partial_value, "tp", scatter_dimension=0, tiled=True)


def kernel(Z, X, Y, C, tok, gain, up, down, out,
           tokg, upg, downg, hid, part, cin, ysum, yin, zlo, zhi, zout, acc,
           wz_s, wz_r, wx_s, wx_r, tu_s, td_s, t_r, ty_s, ty_r, tc_s, tc_r,
           rc_s, rc_r, ry_s, ry_r, rz_s, rlo_r, rhi_r):
    T, D = tok.shape
    F = Z * X
    Dl = up.shape[0]
    B = upg.shape[1]
    fs, tp = lax.axis_index("fs"), lax.axis_index("tp")
    z, x = fs // X, fs % X
    y, c = tp // C, tp % C
    ox, oy, oc = X - 1 - x, Y - 1 - y, C - 1 - c

    def dev(zz=z, xx=x, yy=y, cc=c):
        return {"fs": zz * X + xx, "tp": yy * C + cc}

    def rcopy(src, dst, ss, rs, device):
        return pltpu.make_async_remote_copy(
            src_ref=src, dst_ref=dst, send_sem=ss, recv_sem=rs,
            device_id=device, device_id_type=MESH)

    barrier = pltpu.get_barrier_semaphore()
    peers = [dev(zz=(z + k) % Z) for k in range(1, Z)]
    peers += [dev(xx=ox), dev(yy=oy), dev(cc=oc)]
    for p in peers:
        pl.semaphore_signal(barrier, inc=1, device_id=p, device_id_type=MESH)

    def rows(yy, cc):
        return pl.ds(pl.multiple_of((cc * Y + yy) * T, T), T)

    mine = rows(y, c)

    RB = 32

    @pl.loop(0, T // RB)
    def _(i):
        r = pl.ds(pl.multiple_of(i * RB, RB), RB)
        v = tok[r, :].astype(f32)
        ms = jnp.mean(v * v, axis=-1, keepdims=True)
        w = pl.ds(pl.multiple_of((c * Y + y) * T + i * RB, RB), RB)
        tokg[z, w, :] = (v * lax.rsqrt(ms + epsilon) * gain[...]).astype(bf16)

    pl.semaphore_wait(barrier, len(peers))

    def tok_up(g):
        return rcopy(tokg.at[g, mine], tokg.at[g, mine], tu_s.at[g], t_r.at[g], dev(zz=z + 1))

    def tok_dn(g):
        return rcopy(tokg.at[g, mine], tokg.at[g, mine], td_s.at[g], t_r.at[g], dev(zz=z - 1))

    def tok_y(g):
        return rcopy(tokg.at[g, mine], tokg.at[g, mine], ty_s.at[g], ty_r.at[g], dev(yy=oy))

    def tok_c(g, k):
        w = rows(y if k == 0 else oy, c)
        return rcopy(tokg.at[g, w], tokg.at[g, w], tc_s.at[g, k], tc_r.at[g, k], dev(cc=oc))

    def tok_c_recv(g, k):
        w = rows(y if k == 0 else oy, oc)
        return rcopy(tokg.at[g, w], tokg.at[g, w], tc_s.at[g, k], tc_r.at[g, k], dev(cc=oc))

    def tok_y_recv(g):
        w = rows(oy, c)
        return rcopy(tokg.at[g, w], tokg.at[g, w], ty_s.at[g], ty_r.at[g], dev(yy=oy))

    def up_rows(f):
        return upg.at[pl.ds(pl.multiple_of(f * Dl, Dl), Dl)]

    def wz(zz, k):
        blk = pl.ds(pl.multiple_of(zz * B, B), B)
        if k == 0:
            return rcopy(up.at[:, blk], up_rows(fs), wz_s.at[0, zz], wz_r.at[0, z], dev(zz=zz))
        return rcopy(down.at[blk], downg.at[fs], wz_s.at[1, zz], wz_r.at[1, z], dev(zz=zz))

    def wz_recv(zz, k):
        dst = up_rows(zz * X + x) if k == 0 else downg.at[zz * X + x]
        return rcopy(dst, dst, wz_s.at[k, zz], wz_r.at[k, zz], dev(zz=zz))

    def wx(zz, k):
        dst = up_rows(zz * X + x) if k == 0 else downg.at[zz * X + x]
        return rcopy(dst, dst, wx_s.at[k, zz], wx_r.at[k, zz], dev(xx=ox))

    def wx_recv(zz, k):
        dst = up_rows(zz * X + ox) if k == 0 else downg.at[zz * X + ox]
        return rcopy(dst, dst, wx_s.at[k, zz], wx_r.at[k, zz], dev(xx=ox))

    def wx_own(k):
        blk = pl.ds(pl.multiple_of(z * B, B), B)
        src = up.at[:, blk] if k == 0 else down.at[blk]
        dst = up_rows(fs) if k == 0 else downg.at[fs]
        return rcopy(src, dst, wx_s.at[k, z], wx_r.at[k, z], dev(xx=ox))

    @pl.when(z < Z - 1)
    def _():
        tok_up(z).start()

    @pl.when(z > 0)
    def _():
        tok_dn(z).start()

    tok_y(z).start()
    tok_c(z, 0).start()
    wx_own(0).start()
    wx_own(1).start()
    for d in range(1, Z):
        for sgn in (-1, 1):
            zz = z + sgn * d

            @pl.when((zz >= 0) & (zz < Z))
            def _():
                wz(zz, 0).start()
                wz(zz, 1).start()

    own = pl.ds(pl.multiple_of(z * B, B), B)
    upg[pl.ds(pl.multiple_of(fs * Dl, Dl), Dl), :] = up[:, own]
    downg[fs] = down[own, :]

    def y_forward(g):
        tok_y_recv(g).wait_recv()
        tok_c(g, 1).start()

    for d in range(1, Z + 1):
        for sgn in (-1, 1):
            zz = z + sgn * d
            if d < Z:
                @pl.when((zz >= 0) & (zz < Z))
                def _():
                    tok_up(zz).wait_recv()
                    if sgn < 0:
                        @pl.when(z < Z - 1)
                        def _():
                            tok_up(zz).start()
                    else:
                        @pl.when(z > 0)
                        def _():
                            tok_dn(zz).start()
                    tok_y(zz).start()
                    tok_c(zz, 0).start()
                    for k in range(2):
                        wz_recv(zz, k).wait_recv()
                        wx(zz, k).start()
            if d == 1:
                if sgn > 0:
                    y_forward(z)
            else:
                back = z + sgn * (d - 1)

                @pl.when((back >= 0) & (back < Z))
                def _():
                    y_forward(back)

    for g in range(Z):
        for k in range(2):
            wx_recv(g, k).wait_recv()
            tok_c_recv(g, k).wait_recv()

    table = [sorted(range(Z), key=lambda g, a=a: -abs(g - a)) for a in range(Z)]

    def group(s):
        g = jnp.int32(table[0][s])
        for a in range(1, Z):
            g = jnp.where(z == a, jnp.int32(table[a][s]), g)
        return g

    NB = min(B, 256)

    def compute(g):
        @pl.loop(0, B // NB)
        def _(j):
            cols = pl.ds(pl.multiple_of(j * NB, NB), NB)
            h = jnp.maximum(jnp.dot(tokg[g], upg[:, cols], preferred_element_type=f32), 0.0)
            hid[:, cols] = (h * h).astype(bf16)

        @pl.loop(0, F)
        def _(f):
            cols = pl.ds(pl.multiple_of(f * Dl, Dl), Dl)
            v = jnp.dot(hid[...], downg[f], preferred_element_type=f32).astype(bf16)
            for cc in range(C):
                part[g, cc, :, cols] = v[cc * Y * T:(cc + 1) * Y * T]

    def sum_c(g):
        return rcopy(part.at[g, oc], cin.at[g], rc_s.at[g], rc_r.at[g], dev(cc=oc))

    def sum_y(g):
        return rcopy(ysum.at[g], yin.at[g], ry_s.at[g], ry_r.at[g], dev(yy=oy))

    def sum_up(g):
        return rcopy(zout.at[g], zlo.at[g], rz_s.at[g], rlo_r.at[g], dev(zz=z + 1))

    def sum_dn(g):
        return rcopy(zout.at[g], zhi.at[g], rz_s.at[g], rhi_r.at[g], dev(zz=z - 1))

    def step_y(g):
        sum_c(g).wait_recv()
        r = pl.ds(pl.multiple_of(oy * T, T), T)
        ysum[g] = (part[g, c, r, :].astype(f32) + cin[g, r, :].astype(f32)).astype(bf16)
        sum_y(g).start()

    for s in range(Z):
        g = group(s)
        compute(g)
        sum_c(g).start()
        if s > 0:
            step_y(group(s - 1))
    step_y(group(Z - 1))

    for s in range(Z):
        g = group(s)
        sum_y(g).wait_recv()
        r = pl.ds(pl.multiple_of(y * T, T), T)
        acc[...] = part[g, c, r, :].astype(f32) + cin[g, r, :].astype(f32) + yin[g].astype(f32)

        @pl.when((z <= g) & (z > 0))
        def _():
            sum_up(g).wait_recv()
            acc[...] += zlo[g].astype(f32)

        @pl.when((z >= g) & (z < Z - 1))
        def _():
            sum_dn(g).wait_recv()
            acc[...] += zhi[g].astype(f32)

        @pl.when(z == g)
        def _():
            out[...] = acc[...].astype(bf16)

        @pl.when(z < g)
        def _():
            zout[g] = acc[...].astype(bf16)
            sum_up(g).start()

        @pl.when(z > g)
        def _():
            zout[g] = acc[...].astype(bf16)
            sum_dn(g).start()

    for g in range(Z):
        @pl.when((z < Z - 1) & (g <= z))
        def _():
            tok_up(g).wait_send()

        @pl.when((z > 0) & (g >= z))
        def _():
            tok_dn(g).wait_send()

        tok_y(g).wait_send()
        for k in range(2):
            tok_c(g, k).wait_send()
            wx(g, k).wait_send()

        @pl.when(z != g)
        def _():
            wz(g, 0).wait_send()
            wz(g, 1).wait_send()
            sum_up(g).wait_send()

        sum_c(g).wait_send()
        sum_y(g).wait_send()


def solution(mesh):
    n_fs, n_tp = mesh.shape["fs"], mesh.shape["tp"]
    X = 2 ** (int(math.log2(n_fs)) // 2)
    Z = n_fs // X
    C = 2
    Y = n_tp // C
    placed = (P(("fs", "tp"), None), P(), P("fs", "tp"), P("tp", "fs"))

    def on_device(tokens, norm_gain, up_weight, down_weight):
        T, D = tokens.shape
        Dl, FFl = up_weight.shape
        B = FFl // Z
        if X != 2 or Y != 2 or Z * X != n_fs or Dl % 128 or B % 128 or T % 32:
            return plain(tokens, norm_gain, up_weight, down_weight)
        F = Z * X
        dma = pltpu.SemaphoreType.DMA
        vm = pl.BlockSpec(memory_space=pltpu.VMEM)
        return pl.pallas_call(
            functools.partial(kernel, Z, X, Y, C),
            out_shape=jax.ShapeDtypeStruct((T, D), bf16),
            in_specs=[vm] * 4,
            out_specs=vm,
            scratch_shapes=[
                pltpu.VMEM((Z, C * Y * T, D), bf16),
                pltpu.VMEM((D, B), bf16),
                pltpu.VMEM((F, B, Dl), bf16),
                pltpu.VMEM((C * Y * T, B), bf16),
                pltpu.VMEM((Z, C, Y * T, D), bf16),
                pltpu.VMEM((Z, Y * T, D), bf16),
                pltpu.VMEM((Z, T, D), bf16),
                pltpu.VMEM((Z, T, D), bf16),
                pltpu.VMEM((Z, T, D), bf16),
                pltpu.VMEM((Z, T, D), bf16),
                pltpu.VMEM((Z, T, D), bf16),
                pltpu.VMEM((T, D), f32),
                dma((2, Z)), dma((2, Z)), dma((2, Z)), dma((2, Z)),
                dma((Z,)), dma((Z,)), dma((Z,)), dma((Z,)), dma((Z,)),
                dma((Z, 2)), dma((Z, 2)),
                dma((Z,)), dma((Z,)), dma((Z,)), dma((Z,)),
                dma((Z,)), dma((Z,)), dma((Z,)),
            ],
            compiler_params=pltpu.CompilerParams(
                collective_id=0, has_side_effects=True, vmem_limit_bytes=60 * 2**20),
        )(tokens, norm_gain.reshape(1, D), up_weight, down_weight)

    return jax.shard_map(
        on_device, mesh=mesh, in_specs=placed, out_specs=P(("fs", "tp"), None), check_vma=False)
```

time: 340 us -> 165 us (0.49)
  waiting for transfers between devices: 307 us -> 0 us
  Pallas kernels: 0 us -> 163 us
  matrix products: 16.5 us -> 0 us
  between operations: 13.1 us -> 0.01 us
    all_gather x3 -> x0, waiting for transfers between devices: 276 us -> none  [the longest x1 127 us: on_device(): up_whole = lax.all_gather(up_weight, 'fs', axis=0, tiled=True)]
    pallas_call x0 -> x1, Pallas kernels: none -> 163 us  [on_device(): pl.pallas_call(functools.partial(kernel, Z, X, Y, C), out_shape=jax.Shape...]
    reduce_scatter x1 -> x0, waiting for transfers between devices: 29.5 us -> none  [on_device(): lax.psum_scatter(partial_value.astype(jnp.float32).astype(jnp.bfloat16),...]
    dot_general x1 -> x0, matrix products: 16.5 us -> none  [on_device(): jnp.dot(hidden, down_whole, preferred_element_type=jnp.float32)]
  transfers between devices with their start and end apart: 4 -> 0, of which waited for: 4 -> 0; matrix products, arithmetic and copies ran while one was open for 0% -> 0% of each run, Pallas kernels for 0% -> 0%
where the time goes in v1:
time: 165 us
  Pallas kernels  163 us (99%)
  local copies, waits for them, and re-layouts  1.88 us (1%)
    pallas_call x1, Pallas kernels, on_device(): pl.pallas_call(functools.partial(kernel, Z, X, Y, C), out_shape=jax.Shape...  163 us

profile of v1, /device:TPU:0, one launch (start us, length us, event | category | flops | bytes accessed | tf_op | source)
XLA Modules:
  0.0 164.6 jit_solution(5627078107274185570)
XLA Ops:
  0.0 162.7 %shard_map.46 = bf16[128,2048]{1,0:T(8,128)(2,1)} custom-call(bf16[128,2048]{1,0:T(8,128)(2,1)} %tok.1, f32[1,2048]{1,0:T(1,128)} %bitcast.1, bf16[256,2048]{1,0:T(8,128)(2,1)} %up.1, bf16[2048,256]{1,0:T(8,128)(2,1)} %down.1), custom_call_target="tpu_custom_call" | custom-call | tf_op jit(solution)/shard_map/pallas_call | solution.py:306
  162.7 1.9 %copy.6 = bf16[128,2048]{1,0:T(8,128)(2,1)} copy(bf16[128,2048]{1,0:T(8,128)(2,1)} %shard_map.46) | data formatting | bytes 1048576

commit v2 on v1

v2 whole, which is shorter than its diff:
```python
import functools
import math

import jax
import jax.numpy as jnp
from jax import lax
from jax.experimental import pallas as pl
from jax.experimental.pallas import tpu as pltpu
from jax.sharding import PartitionSpec as P

epsilon = 1e-06
MESH = pl.DeviceIdType.MESH
f32, bf16 = jnp.float32, jnp.bfloat16


def plain(tokens, norm_gain, up_weight, down_weight):
    values = tokens.astype(f32)
    mean_square = jnp.mean(values * values, axis=-1, keepdims=True)
    normed = (values * lax.rsqrt(mean_square + epsilon) * norm_gain).astype(bf16)
    up_whole = lax.all_gather(up_weight, "fs", axis=0, tiled=True)
    rows = lax.all_gather(normed, "tp", axis=0, tiled=True)
    preact = jnp.dot(rows, up_whole, preferred_element_type=f32)
    hidden = jnp.square(jnp.maximum(preact, 0.0)).astype(bf16)
    down_whole = lax.all_gather(down_weight, "fs", axis=1, tiled=True)
    partial_value = jnp.dot(hidden, down_whole, preferred_element_type=f32).astype(bf16)
    return lax.psum_scatter(partial_value, "tp", scatter_dimension=0, tiled=True)


def kernel(Z, X, Y, C, tok, gain, up, down, out,
           tokg, upg, downg, hid, part, cin, zlo, zhi, zout, acc,
           wz_s, wz_r, wx_s, wx_r, wy_s, wy_r, wd_s, wd_r,
           tu_s, td_s, t_r, tc_s, tc_r, rc_s, rc_r, rz_s, rlo_r, rhi_r):
    T, D = tok.shape
    F = Z * X
    Dl = up.shape[0]
    B = upg.shape[2]
    fs, tp = lax.axis_index("fs"), lax.axis_index("tp")
    z, x = fs // X, fs % X
    y, c = tp // C, tp % C
    ox, oy, oc = X - 1 - x, Y - 1 - y, C - 1 - c

    def dev(zz=z, xx=x, yy=y, cc=c):
        return {"fs": zz * X + xx, "tp": yy * C + cc}

    def rcopy(src, dst, ss, rs, device):
        return pltpu.make_async_remote_copy(
            src_ref=src, dst_ref=dst, send_sem=ss, recv_sem=rs,
            device_id=device, device_id_type=MESH)

    barrier = pltpu.get_barrier_semaphore()
    peers = [dev(zz=(z + k) % Z) for k in range(1, Z)]
    peers += [dev(xx=ox), dev(yy=oy), dev(cc=oc)]
    for p in peers:
        pl.semaphore_signal(barrier, inc=1, device_id=p, device_id_type=MESH)

    def rows(cc):
        return pl.ds(pl.multiple_of(cc * T, T), T)

    mine = rows(c)

    RB = 32

    @pl.loop(0, T // RB)
    def _(i):
        r = pl.ds(pl.multiple_of(i * RB, RB), RB)
        v = tok[r, :].astype(f32)
        ms = jnp.mean(v * v, axis=-1, keepdims=True)
        w = pl.ds(pl.multiple_of(c * T + i * RB, RB), RB)
        tokg[z, w, :] = (v * lax.rsqrt(ms + epsilon) * gain[...]).astype(bf16)

    pl.semaphore_wait(barrier, len(peers))

    def tok_up(g):
        return rcopy(tokg.at[g, mine], tokg.at[g, mine], tu_s.at[g], t_r.at[g], dev(zz=z + 1))

    def tok_dn(g):
        return rcopy(tokg.at[g, mine], tokg.at[g, mine], td_s.at[g], t_r.at[g], dev(zz=z - 1))

    def tok_c(g, cc=c):
        w = rows(cc)
        return rcopy(tokg.at[g, w], tokg.at[g, w], tc_s.at[g], tc_r.at[g], dev(cc=oc))

    def piece(zz, xx, yy, k):
        f = zz * X + xx
        if k == 0:
            return upg.at[yy, pl.ds(pl.multiple_of(f * Dl, Dl), Dl)]
        return downg.at[yy, f]

    def own_piece(zz, k):
        blk = pl.ds(pl.multiple_of(zz * B, B), B)
        return up.at[:, blk] if k == 0 else down.at[blk]

    def wz(zz, k):
        return rcopy(own_piece(zz, k), piece(z, x, y, k), wz_s.at[k, zz], wz_r.at[k, z], dev(zz=zz))

    def wz_recv(zz, k):
        p = piece(zz, x, y, k)
        return rcopy(p, p, wz_s.at[k, zz], wz_r.at[k, zz], dev(zz=zz))

    def wx(zz, k, xx=x):
        p = piece(zz, xx, y, k)
        return rcopy(p, p, wx_s.at[k, zz], wx_r.at[k, zz], dev(xx=ox))

    def wy(zz, k, yy=y):
        p = piece(zz, x, yy, k)
        return rcopy(p, p, wy_s.at[k, zz], wy_r.at[k, zz], dev(yy=oy))

    def wd(zz, k):
        if k == 0:
            p = piece(zz, ox, y, 0)
            return rcopy(p, p, wd_s.at[k, zz], wd_r.at[k, zz], dev(yy=oy))
        p = piece(zz, x, oy, 1)
        return rcopy(p, p, wd_s.at[k, zz], wd_r.at[k, zz], dev(xx=ox))

    def wd_recv(zz, k):
        p = piece(zz, ox, oy, k)
        return rcopy(p, p, wd_s.at[k, zz], wd_r.at[k, zz], dev(yy=oy) if k == 0 else dev(xx=ox))

    def each(d, body):
        for sgn in (-1, 1):
            zz = z + sgn * d

            @pl.when((zz >= 0) & (zz < Z))
            def _():
                body(zz, sgn)

    def tokens_out():
        @pl.when(z < Z - 1)
        def _():
            tok_up(z).start()

        @pl.when(z > 0)
        def _():
            tok_dn(z).start()

        tok_c(z).start()

    def weights_out(zz, sgn):
        wz(zz, 0).start()
        wz(zz, 1).start()

    def tokens_on(zz, sgn):
        tok_up(zz).wait_recv()
        if sgn < 0:
            @pl.when(z < Z - 1)
            def _():
                tok_up(zz).start()
        else:
            @pl.when(z > 0)
            def _():
                tok_dn(zz).start()
        tok_c(zz).start()

    def weights_on(zz, sgn):
        for k in range(2):
            wz_recv(zz, k).wait_recv()
            wx(zz, k).start()
            wy(zz, k).start()

    def diagonal(zz, sgn=0):
        wx(zz, 0, ox).wait_recv()
        wd(zz, 0).start()
        wy(zz, 1, oy).wait_recv()
        wd(zz, 1).start()

    def send_own_plane():
        for k in range(2):
            src, dst = own_piece(z, k), piece(z, x, y, k)
            rcopy(src, dst, wx_s.at[k, z], wx_r.at[k, z], dev(xx=ox)).start()
            rcopy(src, dst, wy_s.at[k, z], wy_r.at[k, z], dev(yy=oy)).start()

    def keep_own():
        own = pl.ds(pl.multiple_of(z * B, B), B)
        upg[y, pl.ds(pl.multiple_of(fs * Dl, Dl), Dl), :] = up[:, own]
        downg[y, fs] = down[own, :]

    for d in range(1, Z):
        each(d, weights_out)
    tokens_out()
    send_own_plane()
    keep_own()
    diagonal(z)
    for d in range(1, Z):
        each(d, weights_on)
        if d > 1:
            each(d - 1, diagonal)
            each(d - 1, tokens_on)
    each(Z - 1, diagonal)
    each(Z - 1, tokens_on)

    for g in range(Z):
        for k in range(2):
            wx(g, 1, ox).wait_recv() if k else wy(g, 0, oy).wait_recv()
            wd_recv(g, k).wait_recv()
        tok_c(g, oc).wait_recv()

    table = [sorted(range(Z), key=lambda g, a=a: -abs(g - a)) for a in range(Z)]

    def group(s):
        g = jnp.int32(table[0][s])
        for a in range(1, Z):
            g = jnp.where(z == a, jnp.int32(table[a][s]), g)
        return g

    NB = min(B, 256)

    def compute(g):
        for yy in range(Y):
            @pl.loop(0, B // NB)
            def _(j):
                cols = pl.ds(pl.multiple_of(j * NB, NB), NB)
                h = jnp.maximum(jnp.dot(tokg[g], upg[yy, :, cols], preferred_element_type=f32), 0.0)
                hid[yy, :, cols] = (h * h).astype(bf16)

        @pl.loop(0, F)
        def _(f):
            cols = pl.ds(pl.multiple_of(f * Dl, Dl), Dl)
            v = jnp.dot(hid[0], downg[0, f], preferred_element_type=f32)
            for yy in range(1, Y):
                v = v + jnp.dot(hid[yy], downg[yy, f], preferred_element_type=f32)
            v = v.astype(bf16)
            for cc in range(C):
                part[g, cc, :, cols] = v[cc * T:(cc + 1) * T]

    def sum_c(g):
        return rcopy(part.at[g, oc], cin.at[g], rc_s.at[g], rc_r.at[g], dev(cc=oc))

    def sum_up(g):
        return rcopy(zout.at[g], zlo.at[g], rz_s.at[g], rlo_r.at[g], dev(zz=z + 1))

    def sum_dn(g):
        return rcopy(zout.at[g], zhi.at[g], rz_s.at[g], rhi_r.at[g], dev(zz=z - 1))

    def step_z(g):
        sum_c(g).wait_recv()
        acc[...] = part[g, c].astype(f32) + cin[g].astype(f32)

        @pl.when((z <= g) & (z > 0))
        def _():
            sum_up(g).wait_recv()
            acc[...] += zlo[g].astype(f32)

        @pl.when((z >= g) & (z < Z - 1))
        def _():
            sum_dn(g).wait_recv()
            acc[...] += zhi[g].astype(f32)

        @pl.when(z == g)
        def _():
            out[...] = acc[...].astype(bf16)

        @pl.when(z < g)
        def _():
            zout[g] = acc[...].astype(bf16)
            sum_up(g).start()

        @pl.when(z > g)
        def _():
            zout[g] = acc[...].astype(bf16)
            sum_dn(g).start()

    end = (z == 0) | (z == Z - 1)
    for s in range(Z):
        g = group(s)
        compute(g)
        sum_c(g).start()
        if s > 0:
            @pl.when(end)
            def _():
                step_z(group(s - 1))
    for s in range(Z):
        g = group(s)
        if s < Z - 1:
            @pl.when((z > 0) & (z < Z - 1))
            def _():
                step_z(g)
        else:
            step_z(g)

    for g in range(Z):
        @pl.when((z < Z - 1) & (g <= z))
        def _():
            tok_up(g).wait_send()

        @pl.when((z > 0) & (g >= z))
        def _():
            tok_dn(g).wait_send()

        tok_c(g).wait_send()
        for k in range(2):
            wx(g, k).wait_send()
            wy(g, k).wait_send()
            wd(g, k).wait_send()

        @pl.when(z != g)
        def _():
            wz(g, 0).wait_send()
            wz(g, 1).wait_send()
            sum_up(g).wait_send()

        sum_c(g).wait_send()


def solution(mesh):
    n_fs, n_tp = mesh.shape["fs"], mesh.shape["tp"]
    X = 2 ** (int(math.log2(n_fs)) // 2)
    Z = n_fs // X
    C = 2
    Y = n_tp // C
    placed = (P(("fs", "tp"), None), P(), P("fs", "tp"), P("tp", "fs"))

    def on_device(tokens, norm_gain, up_weight, down_weight):
        T, D = tokens.shape
        Dl, FFl = up_weight.shape
        B = FFl // Z
        if X != 2 or Y != 2 or Z * X != n_fs or Dl % 128 or B % 128 or T % 32:
            return plain(tokens, norm_gain, up_weight, down_weight)
        F = Z * X
        dma = pltpu.SemaphoreType.DMA
        vm = pl.BlockSpec(memory_space=pltpu.VMEM)
        return pl.pallas_call(
            functools.partial(kernel, Z, X, Y, C),
            out_shape=jax.ShapeDtypeStruct((T, D), bf16),
            in_specs=[vm] * 4,
            out_specs=vm,
            scratch_shapes=[
                pltpu.VMEM((Z, C * T, D), bf16),
                pltpu.VMEM((Y, D, B), bf16),
                pltpu.VMEM((Y, F, B, Dl), bf16),
                pltpu.VMEM((Y, C * T, B), bf16),
                pltpu.VMEM((Z, C, T, D), bf16),
                pltpu.VMEM((Z, T, D), bf16),
                pltpu.VMEM((Z, T, D), bf16),
                pltpu.VMEM((Z, T, D), bf16),
                pltpu.VMEM((Z, T, D), bf16),
                pltpu.VMEM((T, D), f32),
                *[dma((2, Z)) for _ in range(8)],
                *[dma((Z,)) for _ in range(10)],
            ],
            compiler_params=pltpu.CompilerParams(
                collective_id=0, has_side_effects=True, vmem_limit_bytes=60 * 2**20),
        )(tokens, norm_gain.reshape(1, D), up_weight, down_weight)

    return jax.shard_map(
        on_device, mesh=mesh, in_specs=placed, out_specs=P(("fs", "tp"), None), check_vma=False)
```

time: 165 us -> 142 us (0.86)
  Pallas kernels: 163 us -> 139 us
    pallas_call x1, Pallas kernels: 163 us -> 139 us  [on_device(): pl.pallas_call(functools.partial(kernel, Z, X, Y, C), out_shape=jax.Shape...]
where the time goes in v2:
time: 142 us; the launch traced here: 141 us
  Pallas kernels  139 us (98%)
  local copies, waits for them, and re-layouts  1.88 us (1%)
    pallas_call x1, Pallas kernels, on_device(): pl.pallas_call(functools.partial(kernel, Z, X, Y, C), out_shape=jax.Shape...  139 us

profile of v2, /device:TPU:0, one launch (start us, length us, event | category | flops | bytes accessed | tf_op | source)
XLA Modules:
  0.0 141.3 jit_solution(12989594642963533075)
XLA Ops:
  0.0 139.4 %shard_map.46 = bf16[128,2048]{1,0:T(8,128)(2,1)} custom-call(bf16[128,2048]{1,0:T(8,128)(2,1)} %tok.1, f32[1,2048]{1,0:T(1,128)} %bitcast.1, bf16[256,2048]{1,0:T(8,128)(2,1)} %up.1, bf16[2048,256]{1,0:T(8,128)(2,1)} %down.1), custom_call_target="tpu_custom_call" | custom-call | tf_op jit(solution)/shard_map/pallas_call | solution.py:321
  139.4 1.9 %copy.6 = bf16[128,2048]{1,0:T(8,128)(2,1)} copy(bf16[128,2048]{1,0:T(8,128)(2,1)} %shard_map.46) | data formatting | bytes 1048576

commit v3 on v2

v3 whole, which is shorter than its diff:
```python
import functools
import math

import jax
import jax.numpy as jnp
from jax import lax
from jax.experimental import pallas as pl
from jax.experimental.pallas import tpu as pltpu
from jax.sharding import PartitionSpec as P

epsilon = 1e-06
MESH = pl.DeviceIdType.MESH
H = 4
f32, bf16 = jnp.float32, jnp.bfloat16


def plain(tokens, norm_gain, up_weight, down_weight):
    values = tokens.astype(f32)
    mean_square = jnp.mean(values * values, axis=-1, keepdims=True)
    normed = (values * lax.rsqrt(mean_square + epsilon) * norm_gain).astype(bf16)
    up_whole = lax.all_gather(up_weight, "fs", axis=0, tiled=True)
    rows = lax.all_gather(normed, "tp", axis=0, tiled=True)
    preact = jnp.dot(rows, up_whole, preferred_element_type=f32)
    hidden = jnp.square(jnp.maximum(preact, 0.0)).astype(bf16)
    down_whole = lax.all_gather(down_weight, "fs", axis=1, tiled=True)
    partial_value = jnp.dot(hidden, down_whole, preferred_element_type=f32).astype(bf16)
    return lax.psum_scatter(partial_value, "tp", scatter_dimension=0, tiled=True)


def kernel(Z, X, Y, C, tok, gain, up, down, out,
           tokg, upg, downg, hid, part, cin, zlo, zhi, zout, acc,
           wz_s, wz_r, wx_s, wx_r, wy_s, wy_r, wd_s, wd_r,
           tu_s, td_s, t_r, tc_s, tc_r, rc_s, rc_r, rz_s, rlo_r, rhi_r):
    T, D = tok.shape
    F = Z * X
    Dl = up.shape[0]
    B = upg.shape[2]
    fs, tp = lax.axis_index("fs"), lax.axis_index("tp")
    z, x = fs // X, fs % X
    y, c = tp // C, tp % C
    ox, oy, oc = X - 1 - x, Y - 1 - y, C - 1 - c

    def dev(zz=z, xx=x, yy=y, cc=c):
        return {"fs": zz * X + xx, "tp": yy * C + cc}

    def rcopy(src, dst, ss, rs, device):
        return pltpu.make_async_remote_copy(
            src_ref=src, dst_ref=dst, send_sem=ss, recv_sem=rs,
            device_id=device, device_id_type=MESH)

    barrier = pltpu.get_barrier_semaphore()
    peers = [dev(zz=(z + k) % Z) for k in range(1, Z)]
    peers += [dev(xx=ox), dev(yy=oy), dev(cc=oc)]
    for p in peers:
        pl.semaphore_signal(barrier, inc=1, device_id=p, device_id_type=MESH)

    def rows(cc):
        return pl.ds(pl.multiple_of(cc * T, T), T)

    mine = rows(c)

    pl.semaphore_wait(barrier, len(peers))

    def tok_up(g):
        return rcopy(tokg.at[g, mine], tokg.at[g, mine], tu_s.at[g], t_r.at[g], dev(zz=z + 1))

    def tok_dn(g):
        return rcopy(tokg.at[g, mine], tokg.at[g, mine], td_s.at[g], t_r.at[g], dev(zz=z - 1))

    def tok_c(g, cc=c):
        w = rows(cc)
        return rcopy(tokg.at[g, w], tokg.at[g, w], tc_s.at[g], tc_r.at[g], dev(cc=oc))

    def piece(zz, xx, yy, k):
        f = zz * X + xx
        if k == 0:
            return upg.at[yy, pl.ds(pl.multiple_of(f * Dl, Dl), Dl)]
        return downg.at[yy, f]

    def own_piece(zz, k):
        blk = pl.ds(pl.multiple_of(zz * B, B), B)
        return up.at[:, blk] if k == 0 else down.at[blk]

    def wz(zz, k):
        return rcopy(own_piece(zz, k), piece(z, x, y, k), wz_s.at[k, zz], wz_r.at[k, z], dev(zz=zz))

    def wz_recv(zz, k):
        p = piece(zz, x, y, k)
        return rcopy(p, p, wz_s.at[k, zz], wz_r.at[k, zz], dev(zz=zz))

    def wx(zz, k, xx=x):
        p = piece(zz, xx, y, k)
        return rcopy(p, p, wx_s.at[k, zz], wx_r.at[k, zz], dev(xx=ox))

    def wy(zz, k, yy=y):
        p = piece(zz, x, yy, k)
        return rcopy(p, p, wy_s.at[k, zz], wy_r.at[k, zz], dev(yy=oy))

    def wd(zz, k):
        if k == 0:
            p = piece(zz, ox, y, 0)
            return rcopy(p, p, wd_s.at[k, zz], wd_r.at[k, zz], dev(yy=oy))
        p = piece(zz, x, oy, 1)
        return rcopy(p, p, wd_s.at[k, zz], wd_r.at[k, zz], dev(xx=ox))

    def wd_recv(zz, k):
        p = piece(zz, ox, oy, k)
        return rcopy(p, p, wd_s.at[k, zz], wd_r.at[k, zz], dev(yy=oy) if k == 0 else dev(xx=ox))

    def each(d, body):
        for sgn in (-1, 1):
            zz = z + sgn * d

            @pl.when((zz >= 0) & (zz < Z))
            def _():
                body(zz, sgn)

    def tokens_out():
        @pl.when(z < Z - 1)
        def _():
            tok_up(z).start()

        @pl.when(z > 0)
        def _():
            tok_dn(z).start()

        tok_c(z).start()

    def weights_out(zz, sgn):
        wz(zz, 0).start()
        wz(zz, 1).start()

    def tokens_on(zz, sgn):
        tok_up(zz).wait_recv()
        if sgn < 0:
            @pl.when(z < Z - 1)
            def _():
                tok_up(zz).start()
        else:
            @pl.when(z > 0)
            def _():
                tok_dn(zz).start()
        tok_c(zz).start()

    def weights_on(zz, sgn):
        for k in range(2):
            wz_recv(zz, k).wait_recv()
            wx(zz, k).start()
            wy(zz, k).start()

    def diagonal(zz, sgn=0):
        wx(zz, 0, ox).wait_recv()
        wd(zz, 0).start()
        wy(zz, 1, oy).wait_recv()
        wd(zz, 1).start()

    def send_own_plane():
        for k in range(2):
            src, dst = own_piece(z, k), piece(z, x, y, k)
            rcopy(src, dst, wx_s.at[k, z], wx_r.at[k, z], dev(xx=ox)).start()
            rcopy(src, dst, wy_s.at[k, z], wy_r.at[k, z], dev(yy=oy)).start()

    def keep_own():
        own = pl.ds(pl.multiple_of(z * B, B), B)
        upg[y, pl.ds(pl.multiple_of(fs * Dl, Dl), Dl), :] = up[:, own]
        downg[y, fs] = down[own, :]

    for d in range(1, Z):
        each(d, weights_out)
    send_own_plane()
    RB = 32

    @pl.loop(0, T // RB)
    def _(i):
        r = pl.ds(pl.multiple_of(i * RB, RB), RB)
        v = tok[r, :].astype(f32)
        ms = jnp.mean(v * v, axis=-1, keepdims=True)
        w = pl.ds(pl.multiple_of(c * T + i * RB, RB), RB)
        tokg[z, w, :] = (v * lax.rsqrt(ms + epsilon) * gain[...]).astype(bf16)

    tokens_out()
    keep_own()
    diagonal(z)
    order = list(range(1, Z))
    for i, d in enumerate(order):
        each(d, weights_on)
        if i > 0:
            each(order[i - 1], diagonal)
            each(i, tokens_on)
    each(order[-1], diagonal)
    each(Z - 1, tokens_on)

    for g in range(Z):
        for k in range(2):
            wx(g, 1, ox).wait_recv() if k else wy(g, 0, oy).wait_recv()
            wd_recv(g, k).wait_recv()
        tok_c(g, oc).wait_recv()

    table = [sorted(range(Z), key=lambda g, a=a: -abs(g - a)) for a in range(Z)]

    def group(s):
        g = jnp.int32(table[0][s])
        for a in range(1, Z):
            g = jnp.where(z == a, jnp.int32(table[a][s]), g)
        return g

    NB = min(B, 256)

    def compute(g):
        for yy in range(Y):
            @pl.loop(0, B // NB)
            def _(j):
                cols = pl.ds(pl.multiple_of(j * NB, NB), NB)
                h = jnp.maximum(jnp.dot(tokg[g], upg[yy, :, cols], preferred_element_type=f32), 0.0)
                hid[yy, :, cols] = (h * h).astype(bf16)

    def project(g, h):
        @pl.loop(h * (F // H), (h + 1) * (F // H))
        def _(f):
            cols = pl.ds(pl.multiple_of(f * Dl, Dl), Dl)
            v = jnp.dot(hid[0], downg[0, f], preferred_element_type=f32)
            for yy in range(1, Y):
                v = v + jnp.dot(hid[yy], downg[yy, f], preferred_element_type=f32)
            v = v.astype(bf16)
            for cc in range(C):
                part[g, cc, :, cols] = v[cc * T:(cc + 1) * T]

    def cut(h):
        return pl.ds(h * (D // H), D // H)

    def sum_c(g, h):
        return rcopy(part.at[g, oc, :, cut(h)], cin.at[g, :, cut(h)], rc_s.at[h, g], rc_r.at[h, g], dev(cc=oc))

    def sum_up(g, h):
        return rcopy(zout.at[g, :, cut(h)], zlo.at[g, :, cut(h)], rz_s.at[h, g], rlo_r.at[h, g], dev(zz=z + 1))

    def sum_dn(g, h):
        return rcopy(zout.at[g, :, cut(h)], zhi.at[g, :, cut(h)], rz_s.at[h, g], rhi_r.at[h, g], dev(zz=z - 1))

    def step_z(g, h):
        w = cut(h)
        sum_c(g, h).wait_recv()
        acc[:, w] = part[g, c, :, w].astype(f32) + cin[g, :, w].astype(f32)

        @pl.when((z <= g) & (z > 0))
        def _():
            sum_up(g, h).wait_recv()
            acc[:, w] += zlo[g, :, w].astype(f32)

        @pl.when((z >= g) & (z < Z - 1))
        def _():
            sum_dn(g, h).wait_recv()
            acc[:, w] += zhi[g, :, w].astype(f32)

        @pl.when(z == g)
        def _():
            out[:, w] = acc[:, w].astype(bf16)

        @pl.when(z < g)
        def _():
            zout[g, :, w] = acc[:, w].astype(bf16)
            sum_up(g, h).start()

        @pl.when(z > g)
        def _():
            zout[g, :, w] = acc[:, w].astype(bf16)
            sum_dn(g, h).start()

    end = (z == 0) | (z == Z - 1)
    items = [(s, h) for s in range(Z) for h in range(H)]
    for i, (s, h) in enumerate(items):
        g = group(s)
        if h == 0:
            compute(g)
        project(g, h)
        sum_c(g, h).start()
        if i > 0 and items[i - 1][0] < Z - 1:
            @pl.when(end)
            def _():
                step_z(group(items[i - 1][0]), items[i - 1][1])
    for s, h in items:
        if s < Z - 1:
            @pl.when((z > 0) & (z < Z - 1))
            def _():
                step_z(group(s), h)
        else:
            step_z(group(s), h)

    for g in range(Z):
        @pl.when((z < Z - 1) & (g <= z))
        def _():
            tok_up(g).wait_send()

        @pl.when((z > 0) & (g >= z))
        def _():
            tok_dn(g).wait_send()

        tok_c(g).wait_send()
        for k in range(2):
            wx(g, k).wait_send()
            wy(g, k).wait_send()
            wd(g, k).wait_send()

        @pl.when(z != g)
        def _():
            wz(g, 0).wait_send()
            wz(g, 1).wait_send()
            for h in range(H):
                sum_up(g, h).wait_send()

        for h in range(H):
            sum_c(g, h).wait_send()


def solution(mesh):
    n_fs, n_tp = mesh.shape["fs"], mesh.shape["tp"]
    X = 2 ** (int(math.log2(n_fs)) // 2)
    Z = n_fs // X
    C = 2
    Y = n_tp // C
    placed = (P(("fs", "tp"), None), P(), P("fs", "tp"), P("tp", "fs"))

    def on_device(tokens, norm_gain, up_weight, down_weight):
        T, D = tokens.shape
        Dl, FFl = up_weight.shape
        B = FFl // Z
        if X != 2 or Y != 2 or Z * X != n_fs or Dl % 128 or B % 128 or T % 32 or D % (128 * H):
            return plain(tokens, norm_gain, up_weight, down_weight)
        F = Z * X
        dma = pltpu.SemaphoreType.DMA
        vm = pl.BlockSpec(memory_space=pltpu.VMEM)
        return pl.pallas_call(
            functools.partial(kernel, Z, X, Y, C),
            out_shape=jax.ShapeDtypeStruct((T, D), bf16),
            in_specs=[vm] * 4,
            out_specs=vm,
            scratch_shapes=[
                pltpu.VMEM((Z, C * T, D), bf16),
                pltpu.VMEM((Y, D, B), bf16),
                pltpu.VMEM((Y, F, B, Dl), bf16),
                pltpu.VMEM((Y, C * T, B), bf16),
                pltpu.VMEM((Z, C, T, D), bf16),
                pltpu.VMEM((Z, T, D), bf16),
                pltpu.VMEM((Z, T, D), bf16),
                pltpu.VMEM((Z, T, D), bf16),
                pltpu.VMEM((Z, T, D), bf16),
                pltpu.VMEM((T, D), f32),
                *[dma((2, Z)) for _ in range(8)],
                *[dma((Z,)) for _ in range(5)],
                *[dma((H, Z)) for _ in range(5)],
            ],
            compiler_params=pltpu.CompilerParams(
                collective_id=0, has_side_effects=True, vmem_limit_bytes=60 * 2**20),
        )(tokens, norm_gain.reshape(1, D), up_weight, down_weight)

    return jax.shard_map(
        on_device, mesh=mesh, in_specs=placed, out_specs=P(("fs", "tp"), None), check_vma=False)
```

time: 142 us -> 130 us (0.915)
  Pallas kernels: 139 us -> 128 us
    pallas_call x1, Pallas kernels: 139 us -> 128 us  [on_device(): pl.pallas_call(functools.partial(kernel, Z, X, Y, C), out_shape=jax.Shape...]
where the time goes in v3:
time: 130 us
  Pallas kernels  128 us (98%)
  local copies, waits for them, and re-layouts  1.88 us (1%)
    pallas_call x1, Pallas kernels, on_device(): pl.pallas_call(functools.partial(kernel, Z, X, Y, C), out_shape=jax.Shape...  128 us

profile of v3, /device:TPU:0, one launch (start us, length us, event | category | flops | bytes accessed | tf_op | source)
XLA Modules:
  0.0 130.1 jit_solution(7225959465469153157)
XLA Ops:
  0.0 128.2 %shard_map.46 = bf16[128,2048]{1,0:T(8,128)(2,1)} custom-call(bf16[128,2048]{1,0:T(8,128)(2,1)} %tok.1, f32[1,2048]{1,0:T(1,128)} %bitcast.1, bf16[256,2048]{1,0:T(8,128)(2,1)} %up.1, bf16[2048,256]{1,0:T(8,128)(2,1)} %down.1), custom_call_target="tpu_custom_call" | custom-call | tf_op jit(solution)/shard_map/pallas_call | solution.py:332
  128.2 1.9 %copy.6 = bf16[128,2048]{1,0:T(8,128)(2,1)} copy(bf16[128,2048]{1,0:T(8,128)(2,1)} %shard_map.46) | data formatting | bytes 1048576
